TPU v7x, 32 devices: a whole 2x2x4 slice. The times are simulated.
32 devices in a mesh: sp: 8 (over z, y), tp: 4 (over x, core).
Axes of the slice: x: 2, y: 2, z: 4, core: 2. Of those that a mesh axis runs over, the one named last changes fastest.
Arguments:
- residual_in: bfloat16 [8192, 2048], P(('sp', 'tp')), may hold values from -6 to 6
- queries: bfloat16 [8192, 2048], P('sp', 'tp'), may hold values from -200 to 200, as said below
- keys_values: bfloat16 [2, 8192, 1024], P(None, 'sp', 'tp'), may hold values from -6 to 6
- sink_logit: float32 [32], P('tp'), may hold values from -2 to 6
- out_weight: bfloat16 [2048, 2048], P('tp'), may hold values from -2 to 2
- norm1_gain: float32 [2048], replicated, may hold values from 0.1 to 1.9
- norm1_bias: float32 [2048], replicated, may hold values from -3 to 3
- up_weight: bfloat16 [2048, 8192], P('sp', 'tp'), may hold values from -0.125 to 0.125
- down_weight: bfloat16 [8192, 2048], P('tp', 'sp'), may hold values from -0.0625 to 0.0625
- norm2_gain: float32 [2048], replicated, may hold values from 0.1 to 1.9
- norm2_bias: float32 [2048], replicated, may hold values from -3 to 3
Outputs:
- stream_out: bfloat16 [8192, 2048], P(('sp', 'tp'))
Inputs may be any that keep to these rules, and one draw needn't show every extreme that they name: `queries`: of order one mostly; some rows may be large multiples of a nearby key row.
All inputs are finite; a program needn't handle non-finite values.
Results may differ from a plain program's by a relative error of at most 0.014.
Values may be sent and summed in bfloat16 or wider, within the bound.
A program may use at most 128 MiB of HBM per device.

v0:
```python
import jax
import jax.numpy as jnp
from jax import lax
from jax.sharding import PartitionSpec as P

HEAD_DIM = 64
WINDOW = 128


def with_halo(shard, sides, width):
    for axis, dim in sides:
        devices, length = (lax.axis_size(axis), shard.shape[dim])
        up = [(i, (i + 1) % devices) for i in range(devices - 1)]
        down = [(j, i) for i, j in up]
        last = lax.slice_in_dim(shard, length - width, length, axis=dim)
        first = lax.slice_in_dim(shard, 0, width, axis=dim)
        before = lax.ppermute(last, axis, up)
        after = lax.ppermute(first, axis, down)
        shard = jnp.concatenate([before, shard, after], axis=dim)
    return shard


def norm_rows(values, gain, bias):
    mean = jnp.mean(values, axis=-1, keepdims=True)
    centred = values - mean
    variance = jnp.mean(centred * centred, axis=-1, keepdims=True)
    return (centred * lax.rsqrt(variance + 1e-06) * gain + bias).astype(jnp.bfloat16)


def attend(queries, padded, sink_logit, offset, total):
    tok_rows = queries.shape[0]
    block = min(512, tok_rows)
    span = block + 2 * WINDOW
    kv_local = padded.shape[2] // HEAD_DIM
    heads_local = queries.shape[1] // HEAD_DIM
    group = heads_local // kv_local
    sink = sink_logit.reshape(kv_local, group, 1, 1)

    def one_block(index):
        start = index * block
        query = lax.dynamic_slice_in_dim(queries, start, block, 0).reshape(
            block, kv_local, group, HEAD_DIM
        )
        keys = lax.dynamic_slice_in_dim(padded[0], start, span, 0).reshape(span, kv_local, HEAD_DIM)
        values = lax.dynamic_slice_in_dim(padded[1], start, span, 0).reshape(
            span, kv_local, HEAD_DIM
        )
        scores = jnp.einsum(
            "qhgd,khd->hgqk", query, keys, preferred_element_type=jnp.float32
        ) * HEAD_DIM ** (-0.5)
        query_pos = offset + start + jnp.arange(block, dtype=jnp.int32)
        key_pos = offset + start - WINDOW + jnp.arange(span, dtype=jnp.int32)
        valid = (
            (jnp.abs(key_pos[None, :] - query_pos[:, None]) <= WINDOW)
            & (key_pos[None, :] >= 0)
            & (key_pos[None, :] < total)
        )
        scores = jnp.where(valid, scores, -jnp.inf)
        top = jnp.maximum(jnp.max(scores, axis=-1, keepdims=True), sink)
        expd = jnp.exp(scores - top)
        denom = jnp.sum(expd, axis=-1, keepdims=True) + jnp.exp(sink - top)
        weights = (expd / denom).astype(jnp.bfloat16)
        mixed = jnp.einsum("hgqk,khd->qhgd", weights, values, preferred_element_type=jnp.float32)
        return mixed.reshape(block, heads_local * HEAD_DIM).astype(jnp.bfloat16)

    blocks = lax.map(one_block, jnp.arange(tok_rows // block, dtype=jnp.int32))
    return blocks.reshape(tok_rows, heads_local * HEAD_DIM)


def activate(rows, up_full):
    hidden = jnp.dot(rows, up_full, preferred_element_type=jnp.float32)
    return jnp.square(jnp.maximum(hidden, 0.0)).astype(jnp.bfloat16)


def on_device(
    residual_in,
    queries,
    keys_values,
    sink_logit,
    out_weight,
    norm1_gain,
    norm1_bias,
    up_weight,
    down_weight,
    norm2_gain,
    norm2_bias,
):
    up_full, down_full = (
        lax.all_gather(up_weight, "sp", axis=0, tiled=True),
        lax.all_gather(down_weight, "sp", axis=1, tiled=True),
    )
    tok_rows = queries.shape[0]
    padded = with_halo(keys_values, (("sp", 1),), WINDOW)
    offset = lax.axis_index("sp") * tok_rows
    attended = attend(queries, padded, sink_logit, offset, tok_rows * lax.axis_size("sp"))
    rows = attended
    projected = lax.psum_scatter(
        jnp.dot(rows, out_weight, preferred_element_type=jnp.float32)
        .astype(jnp.bfloat16)
        .astype(jnp.float32)
        .astype(jnp.bfloat16),
        "tp",
        scatter_dimension=0,
        tiled=True,
    ).astype(jnp.float32)
    first = norm_rows(residual_in.astype(jnp.float32) + projected, norm1_gain, norm1_bias)
    activation = activate(lax.all_gather(first, "tp", axis=0, tiled=True), up_full)
    rows = activation
    branch = lax.psum_scatter(
        jnp.dot(rows, down_full, preferred_element_type=jnp.float32)
        .astype(jnp.bfloat16)
        .astype(jnp.float32)
        .astype(jnp.bfloat16),
        "tp",
        scatter_dimension=0,
        tiled=True,
    ).astype(jnp.float32)
    return norm_rows(first.astype(jnp.float32) + branch, norm2_gain, norm2_bias)


def solution(mesh):
    return jax.shard_map(
        on_device,
        mesh=mesh,
        in_specs=(
            P(("sp", "tp"), None),
            P("sp", "tp"),
            P(None, "sp", "tp"),
            P("tp"),
            P("tp", None),
            P(),
            P(),
            P("sp", "tp"),
            P("tp", "sp"),
            P(),
            P(),
        ),
        out_specs=P(("sp", "tp"), None),
        check_vma=False,
    )
```

profile of v0, /device:TPU:0, one launch (start us, length us, event | category | flops | bytes accessed | tf_op | source)
XLA Modules:
  0.0 449.1 jit_solution(10335722248176665415)
XLA Ops:
  7.4 1.6 copy.21
  9.0 0.7 fusion.16
  9.7 4.9 %collective-permute-start = (bf16[2,128,256]{1,2,0:T(8,128)(2,1)}, bf16[2,128,256]{1,2,0:T(8,128)(2,1)S(1)}, u32[]{:S(2)}, u32[]{:S(2)}) collective-permute-start(bf16[2,128,256]{1,2,0:T(8,128)(2,1)} %get-tuple-element.131), channel_id=1, source_target_pairs={{0,4},{4,8},{8,12},{12,16},{16,20},{20,24},{24,28},{1,5},{5,9},{9,... | collective-permute-start | bytes 393224 | tf_op jit(solution)/shard_map/ppermute | solution.py:17
  14.6 1.3 collective-permute-start.1
  15.9 0.1 reshape.111
  16.0 0.1 copy.25
  16.1 1.5 collective-permute-done
  17.7 3.8 collective-permute-done.1
  21.5 1.2 pad_maximum_fusion
  22.7 52.6 %while.12 = (s32[]{:T(128)}, bf16[2,512,512]{2,1,0:T(8,128)(2,1)}, bf16[2,1280,256]{1,2,0:T(8,128)(2,1)}, s32[2]{0:T(128)S(1)}, s32[]{:T(128)}, /*index=5*/bf16[...) while((s32[]{:T(128)}, bf16[2,512,512]{2,1,0:T(8,128)(2,1)}, ...), condition=%wide.region_3.4_spmd, body=%wide.region_0.3_spmd.sunk | while | flops 845295104 | bytes 101627824 | solution.py:66
  22.7 0.6 dynamic_slice.27
  24.0 0.8 fusion.39
  24.8 1.4 fusion.37
  26.2 1.0 constant_dynamic-slice_fusion.5
  27.2 1.1 constant_dynamic-slice_fusion.6
  28.2 0.2 copy.36
  28.5 7.6 %fusion.40 = (f32[4,2,512]{2,1,0:T(2,128)S(1)}, f32[4,768,512,2]{2,1,3,0:T(8,128)}) fusion(pred[512,768]{0,1:T(8,128)(4,1)S(1)} %fusion.39, bf16[768,4,64,1]{0,2,3,1:T(8,128)(2,1)} %bitcast.61, bf16[512,4,2,64]{0,3,2,1:T(8,128)(2,1)S(1)} %bitcast.60), kind=kOutput, calls=%fused_computation.4.clone.1 | convolution fusion | flops 412086272 | bytes 13910016 | tf_op jit(solution)/shard_map/while/body/eval_jaxpr/qhgd,khd->hgqk/dot_general | solution.py:48
  36.1 0.1 copy.37
  36.2 0.1 broadcast_maximum_fusion.2
  36.2 7.3 %fusion.41 = f32[4,2,512]{2,1,0:T(2,128)S(1)} fusion(f32[4,768,512,2]{2,1,3,0:T(8,128)} %get-tuple-element.190, f32[4,2,512]{2,1,0:T(2,128)S(1)} %broadcast_maximum_fusion.2, pred[512,768]{0,1:T(8,128)(4,1)S(1)} %fusion.39), kind=kLoop, calls=%fused_computation.3.clone.1 | loop fusion | flops 12578816 | bytes 13008896 | tf_op jit(solution)/shard_map/while/body/eval_jaxpr/reduce_sum | solution.py:61
  43.6 0.1 exponential_add_fusion.2
  43.7 0.7 copy-done.1
  44.4 3.6 fusion.42
  48.0 0.2 copy.38
  48.2 0.8 constant_dynamic-update-slice_fusion.2
  49.0 0.6 dynamic_slice.27
  50.3 0.8 fusion.39
  51.1 1.4 fusion.37
  52.5 1.0 constant_dynamic-slice_fusion.5
  53.5 1.1 constant_dynamic-slice_fusion.6
  54.5 0.2 copy.36
  54.8 7.6 %fusion.40 = (f32[4,2,512]{2,1,0:T(2,128)S(1)}, f32[4,768,512,2]{2,1,3,0:T(8,128)}) fusion(pred[512,768]{0,1:T(8,128)(4,1)S(1)} %fusion.39, bf16[768,4,64,1]{0,2,3,1:T(8,128)(2,1)} %bitcast.61, bf16[512,4,2,64]{0,3,2,1:T(8,128)(2,1)S(1)} %bitcast.60), kind=kOutput, calls=%fused_computation.4.clone.1 | convolution fusion | flops 412086272 | bytes 13910016 | tf_op jit(solution)/shard_map/while/body/eval_jaxpr/qhgd,khd->hgqk/dot_general | solution.py:48
  62.4 0.1 copy.37
  62.5 0.1 broadcast_maximum_fusion.2
  62.5 7.3 %fusion.41 = f32[4,2,512]{2,1,0:T(2,128)S(1)} fusion(f32[4,768,512,2]{2,1,3,0:T(8,128)} %get-tuple-element.190, f32[4,2,512]{2,1,0:T(2,128)S(1)} %broadcast_maximum_fusion.2, pred[512,768]{0,1:T(8,128)(4,1)S(1)} %fusion.39), kind=kLoop, calls=%fused_computation.3.clone.1 | loop fusion | flops 12578816 | bytes 13008896 | tf_op jit(solution)/shard_map/while/body/eval_jaxpr/reduce_sum | solution.py:61
  69.9 0.1 exponential_add_fusion.2
  70.0 0.7 copy-done.1
  70.7 3.6 fusion.42
  74.3 0.2 copy.38
  74.5 0.8 constant_dynamic-update-slice_fusion.2
  75.3 5.5 %convolution_convert_fusion.1 = bf16[1024,2048]{1,0:T(8,128)(2,1)} fusion(bf16[1024,512]{1,0:T(8,128)(2,1)} %bitcast.65, bf16[512,2048]{1,0:T(8,128)(2,1)S(1)} %copy-done), kind=kOutput, calls=%fused_computation.24 | convolution fusion | flops 2149580800 | bytes 7340032 | tf_op jit(solution)/shard_map/dot_general | solution.py:98
  80.9 0.0 reduce-scatter.3.cloned.1.call-update
  80.9 0.0 all-gather.6.cloned.1.call-start
  80.9 0.5 all-gather.6.cloned.1.call-update
  81.5 0.0 copy-start.7
  81.5 0.0 all-gather.8.cloned.1.call-start
  81.5 0.5 all-gather.8.cloned.1.call-update
  82.1 0.0 all-gather.4.cloned.1.call-start
  82.1 44.6 %reduce-scatter.3.cloned.1.call-done = bf16[256,2048]{1,0:T(8,128)(2,1)} async-done(((bf16[1024,2048]{1,0:T(8,128)(2,1)}), bf16[256,2048]{1,0:T(8,128)(2,1)}) %reduce-scatter.3.cloned.1.call-update) | async-done | bytes 1048592 | tf_op jit(solution)/shard_map/reduce_scatter | solution.py:97
  126.7 1.7 fusion.11
  128.4 0.5 multiply_reduce_fusion.1
  129.0 1.5 add_convert_fusion.1
  130.5 0.0 all-gather.4.cloned.1.call-update
  130.5 0.2 reduce-scatter.5.cloned.1.call-start
  130.8 78.1 %all-gather.6.cloned.1.call-done = bf16[2048,2048]{1,0:T(8,128)(2,1)} async-done(((bf16[256,2048]{1,0:T(8,128)(2,1)}), bf16[2048,2048]{1,0:T(8,128)(2,1)}) %all-gather.6.cloned.1.call-update) | async-done | bytes 8388624 | tf_op jit(solution)/shard_map/all_gather | solution.py:89
  208.8 124.8 %all-gather.8.cloned.1.call-done = bf16[2048,2048]{1,0:T(8,128)(2,1)} async-done(((bf16[2048,256]{1,0:T(8,128)(2,1)}), bf16[2048,2048]{1,0:T(8,128)(2,1)}) %all-gather.8.cloned.1.call-update) | async-done | bytes 8388624 | tf_op jit(solution)/shard_map/all_gather | solution.py:90
  333.7 34.0 %all-gather.4.cloned.1.call-done = bf16[1024,2048]{1,0:T(8,128)(2,1)} async-done(((bf16[256,2048]{1,0:T(8,128)(2,1)}), bf16[1024,2048]{1,0:T(8,128)(2,1)}) %all-gather.4.cloned.1.call-update) | async-done | bytes 4194320 | tf_op jit(solution)/shard_map/all_gather | solution.py:107
  367.6 25.4 %convolution_convert_fusion = bf16[1024,2048]{1,0:T(8,128)(2,1)} fusion(bf16[2048,2048]{1,0:T(8,128)(2,1)} %all-gather.8.cloned.1.call-done, bf16[1024,2048]{1,0:T(8,128)(2,1)} %all-gather.4.cloned.1.call-done, bf16[2048,2048]{1,0:T(8,128)(2,1)} %all-gather.6.cloned.1.call-done), kind=kOutput, calls=%fused_computation.23 | convolution fusion | flops 17188257792 | bytes 25165824 | tf_op jit(solution)/shard_map/dot_general | solution.py:110
  393.0 0.0 reduce-scatter.5.cloned.1.call-update
  393.0 0.0 copy-start.10
  393.0 44.7 %reduce-scatter.5.cloned.1.call-done = bf16[256,2048]{1,0:T(8,128)(2,1)} async-done(((bf16[1024,2048]{1,0:T(8,128)(2,1)}), bf16[256,2048]{1,0:T(8,128)(2,1)}) %reduce-scatter.5.cloned.1.call-update) | async-done | bytes 1048592 | tf_op jit(solution)/shard_map/reduce_scatter | solution.py:109
  437.8 1.7 fusion.13
  439.5 0.5 multiply_reduce_fusion
  440.0 1.5 add_convert_fusion
  (37 shorter events, 0.1 us)
Async XLA Ops:
  7.4 68.0 %copy-start = (bf16[512,2048]{1,0:T(8,128)(2,1)S(1)}, bf16[512,2048]{1,0:T(8,128)(2,1)}, u32[]{:S(2)}) copy-start(bf16[512,2048]{1,0:T(8,128)(2,1)} %param.17) | copy-start | bytes 6291460
  7.4 8.6 %copy-start.11 = (f32[8]{0:T(128)S(1)}, f32[8]{0:T(128)}, u32[]{:S(2)}) copy-start(f32[8]{0:T(128)} %param.16) | copy-start | bytes 100
  7.4 119.3 %reduce-scatter.3.cloned.1.call-start = ((), (), s32[]{:S(2)}) async-start(), calls=%async_computation.2 | async-start | bytes 5242880 | tf_op jit(solution)/shard_map/reduce_scatter | solution.py:97
  9.7 7.9 %collective-permute-start = (bf16[2,128,256]{1,2,0:T(8,128)(2,1)}, bf16[2,128,256]{1,2,0:T(8,128)(2,1)S(1)}, u32[]{:S(2)}, u32[]{:S(2)}) collective-permute-start(bf16[2,128,256]{1,2,0:T(8,128)(2,1)} %get-tuple-element.131), channel_id=1, source_target_pairs={{0,4},{4,8},{8,12},{12,16},{16,20},{20,24},{24,28},{1,5},{5,9},{9,... | collective-permute-start | bytes 393224 | tf_op jit(solution)/shard_map/ppermute | solution.py:17
  14.6 6.9 %collective-permute-start.1 = (bf16[2,128,256]{1,2,0:T(8,128)(2,1)S(1)}, bf16[2,128,256]{1,2,0:T(8,128)(2,1)S(1)}, u32[]{:S(2)}, u32[]{:S(2)}) collective-permute-start(bf16[2,128,256]{1,2,0:T(8,128)(2,1)S(1)} %get-tuple-element.132), channel_id=1, source_target_pairs={{4,0},{8,4},{12,8},{16,12},{20,16},{24,20},{28,24},{5,1},{9,5},{13... | collective-permute-start | bytes 393224 | tf_op jit(solution)/shard_map/ppermute | solution.py:18
  36.2 8.2 %copy-start.1 = (f32[4,768,512,2]{2,1,3,0:T(8,128)S(1)}, f32[4,768,512,2]{2,1,3,0:T(8,128)}, u32[]{:S(2)}) copy-start(f32[4,768,512,2]{2,1,3,0:T(8,128)} %get-tuple-element.190) | copy-start | bytes 37748740 | tf_op jit(solution)/shard_map/while
  36.2 8.2 %copy-start.3 = (bf16[1,768,256]{1,2,0:T(8,128)(2,1)S(1)}, bf16[1,768,256]{1,2,0:T(8,128)(2,1)}, u32[]{:S(2)}) copy-start(bf16[1,768,256]{1,2,0:T(8,128)(2,1)} %get-tuple-element.186) | copy-start | bytes 1179652 | tf_op jit(solution)/shard_map/while
  62.5 8.2 %copy-start.1 = (f32[4,768,512,2]{2,1,3,0:T(8,128)S(1)}, f32[4,768,512,2]{2,1,3,0:T(8,128)}, u32[]{:S(2)}) copy-start(f32[4,768,512,2]{2,1,3,0:T(8,128)} %get-tuple-element.190) | copy-start | bytes 37748740 | tf_op jit(solution)/shard_map/while
  62.5 8.2 %copy-start.3 = (bf16[1,768,256]{1,2,0:T(8,128)(2,1)S(1)}, bf16[1,768,256]{1,2,0:T(8,128)(2,1)}, u32[]{:S(2)}) copy-start(bf16[1,768,256]{1,2,0:T(8,128)(2,1)} %get-tuple-element.186) | copy-start | bytes 1179652 | tf_op jit(solution)/shard_map/while
  80.8 45.9 %copy-start.4 = (bf16[256,2048]{1,0:T(8,128)(2,1)S(1)}, bf16[256,2048]{1,0:T(8,128)(2,1)}, u32[]{:S(2)}) copy-start(bf16[256,2048]{1,0:T(8,128)(2,1)} %param.13) | copy-start | bytes 3145732
  80.9 127.9 %all-gather.6.cloned.1.call-start = ((), (), s32[]{:S(2)}) async-start(), calls=%async_computation.4 | async-start | bytes 9437184 | tf_op jit(solution)/shard_map/all_gather | solution.py:89
  81.5 47.5 %copy-start.7 = (f32[2048]{0:T(1024)S(1)}, f32[2048]{0:T(1024)}, u32[]{:S(2)}) copy-start(f32[2048]{0:T(1024)} %param.19) | copy-start | bytes 24580
  81.5 47.5 %copy-start.8 = (f32[2048]{0:T(1024)S(1)}, f32[2048]{0:T(1024)}, u32[]{:S(2)}) copy-start(f32[2048]{0:T(1024)} %param.18) | copy-start | bytes 24580
  81.5 252.2 %all-gather.8.cloned.1.call-start = ((), (), s32[]{:S(2)}) async-start(), calls=%async_computation.5 | async-start | bytes 9437184 | tf_op jit(solution)/shard_map/all_gather | solution.py:90
  82.1 285.5 %all-gather.4.cloned.1.call-start = ((), (), s32[]{:S(2)}) async-start(), calls=%async_computation.3 | async-start | bytes 5242880 | tf_op jit(solution)/shard_map/all_gather | solution.py:107
  126.7 1.7 copy-start.5
  130.5 307.3 %reduce-scatter.5.cloned.1.call-start = ((), (), s32[]{:S(2)}) async-start(), calls=%async_computation.6 | async-start | bytes 5242880 | tf_op jit(solution)/shard_map/reduce_scatter | solution.py:109
  393.0 44.8 %copy-start.2 = (bf16[256,2048]{1,0:T(8,128)(2,1)S(1)}, bf16[256,2048]{1,0:T(8,128)(2,1)}, u32[]{:S(2)}) copy-start(bf16[256,2048]{1,0:T(8,128)(2,1)} %add_convert_fusion.1) | copy-start | bytes 3145732
  393.0 47.0 %copy-start.9 = (f32[2048]{0:T(1024)S(1)}, f32[2048]{0:T(1024)}, u32[]{:S(2)}) copy-start(f32[2048]{0:T(1024)} %param.23) | copy-start | bytes 24580
  393.0 47.0 %copy-start.10 = (f32[2048]{0:T(1024)S(1)}, f32[2048]{0:T(1024)}, u32[]{:S(2)}) copy-start(f32[2048]{0:T(1024)} %param.22) | copy-start | bytes 24580
  437.8 1.7 copy-start.6
Sparse Core Ops, SparseCore 0:
  81.0 45.6 reduce-scatter.2
  393.1 44.5 reduce-scatter.4
Sparse Core Ops, SparseCore 1:
  83.5 125.3 all-gather.5
  210.7 122.9 all-gather.7
  335.1 32.5 all-gather.3
where the time goes:
time: 450 us; the launch traced here: 449 us
  waiting for transfers between devices  333 us (74%)
  matrix products  53.3 us (12%)
  other arithmetic  25.3 us (6%)
  between operations  15.2 us (3%)
  local copies, waits for them, and re-layouts  14.8 us (3%)
  starting transfers between devices  6.54 us (1%)
    all_gather x1, waiting for transfers between devices, on_device(): lax.all_gather(down_weight, 'sp', axis=1, tiled=True)  125 us
    all_gather x1, waiting for transfers between devices, on_device(): lax.all_gather(up_weight, 'sp', axis=0, tiled=True)  78.1 us
    reduce_scatter x1, waiting for transfers between devices, on_device(): lax.psum_scatter(jnp.dot(rows, down_full, preferred_element_type=jnp.floa...  44.7 us
    reduce_scatter x1, waiting for transfers between devices, on_device(): lax.psum_scatter(jnp.dot(rows, out_weight, preferred_element_type=jnp.flo...  44.6 us
    all_gather x1, waiting for transfers between devices, on_device(): lax.all_gather(first, 'tp', axis=0, tiled=True)  34 us
    dot_general x1, matrix products, on_device(): jnp.dot(rows, down_full, preferred_element_type=jnp.float32)  25.4 us
    dot_general x2, matrix products, one_block(): jnp.einsum('qhgd,khd->hgqk', query, keys, preferred_element_type=jnp.floa...  15.2 us
    reduce_sum x2, other arithmetic, one_block(): denom = jnp.sum(expd, axis=-1, keepdims=True) + jnp.exp(sink - top)  14.7 us
  transfers between devices with their start and end apart: 7, of which 7 were waited for; matrix products, arithmetic and copies ran while one was open for 1% of the time, Pallas kernels for 0%

commit v1 on v0

--- a/solution.py
+++ b/solution.py
@@ -87,7 +87,7 @@
 ):
     up_full, down_full = (
         lax.all_gather(up_weight, "sp", axis=0, tiled=True),
-        lax.all_gather(down_weight, "sp", axis=1, tiled=True),
+        jnp.concatenate(lax.all_gather(down_weight, "sp"), axis=1),
     )
     tok_rows = queries.shape[0]
     padded = with_halo(keys_values, (("sp", 1),), WINDOW)

time: 450 us -> 449 us (level)
  waiting for transfers between devices: 333 us -> 320 us
  local copies, waits for them, and re-layouts: 14.8 us -> 26.6 us
    all_gather x1, waiting for transfers between devices: 125 us -> 78.1 us  [on_device(): lax.all_gather(down_weight, 'sp')]
    all_gather x1, waiting for transfers between devices: 78.1 us -> 113 us  [on_device(): lax.all_gather(up_weight, 'sp', axis=0, tiled=True)]
    reshape x0 -> x1, local copies, waits for them, and re-layouts: none -> 11.7 us  [on_device(): jnp.concatenate(lax.all_gather(down_weight, 'sp'), axis=1)]
  transfers between devices with their start and end apart: 7 -> 7, of which waited for: 7 -> 7; matrix products, arithmetic and copies ran while one was open for 1% -> 3% of each run, Pallas kernels for 0% -> 0%
where the time goes in v1:
time: 449 us
  waiting for transfers between devices  320 us (71%)
  matrix products  53.3 us (12%)
  local copies, waits for them, and re-layouts  26.6 us (6%)
  other arithmetic  25.3 us (6%)
  between operations  15.2 us (3%)
  starting transfers between devices  6.54 us (1%)
    all_gather x1, waiting for transfers between devices, on_device(): lax.all_gather(up_weight, 'sp', axis=0, tiled=True)  113 us
    all_gather x1, waiting for transfers between devices, on_device(): lax.all_gather(down_weight, 'sp')  78.1 us
    reduce_scatter x1, waiting for transfers between devices, on_device(): lax.psum_scatter(jnp.dot(rows, down_full, preferred_element_type=jnp.floa...  44.7 us
    reduce_scatter x1, waiting for transfers between devices, on_device(): lax.psum_scatter(jnp.dot(rows, out_weight, preferred_element_type=jnp.flo...  44.6 us
    all_gather x1, waiting for transfers between devices, on_device(): lax.all_gather(first, 'tp', axis=0, tiled=True)  34 us
    dot_general x1, matrix products, on_device(): jnp.dot(rows, down_full, preferred_element_type=jnp.float32)  25.4 us
    dot_general x2, matrix products, one_block(): jnp.einsum('qhgd,khd->hgqk', query, keys, preferred_element_type=jnp.floa...  15.2 us
    reduce_sum x2, other arithmetic, one_block(): denom = jnp.sum(expd, axis=-1, keepdims=True) + jnp.exp(sink - top)  14.7 us
  transfers between devices with their start and end apart: 7, of which 7 were waited for; matrix products, arithmetic and copies ran while one was open for 3% of the time, Pallas kernels for 0%

profile of v1, /device:TPU:0, one launch (start us, length us, event | category | flops | bytes accessed | tf_op | source)
XLA Modules:
  0.0 448.6 jit_solution(3657825355428759963)
XLA Ops:
  7.4 1.6 copy.29
  9.0 0.7 fusion.16
  9.7 4.9 %collective-permute-start = (bf16[2,128,256]{1,2,0:T(8,128)(2,1)}, bf16[2,128,256]{1,2,0:T(8,128)(2,1)S(1)}, u32[]{:S(2)}, u32[]{:S(2)}) collective-permute-start(bf16[2,128,256]{1,2,0:T(8,128)(2,1)} %get-tuple-element.138), channel_id=1, source_target_pairs={{0,4},{4,8},{8,12},{12,16},{16,20},{20,24},{24,28},{1,5},{5,9},{9,... | collective-permute-start | bytes 393224 | tf_op jit(solution)/shard_map/ppermute | solution.py:17
  14.6 1.3 collective-permute-start.1
  15.9 0.1 reshape.117
  16.0 0.1 copy.33
  16.1 1.5 collective-permute-done
  17.7 3.8 collective-permute-done.1
  21.5 1.2 pad_maximum_fusion
  22.7 52.6 %while.12 = (s32[]{:T(128)}, bf16[2,512,512]{2,1,0:T(8,128)(2,1)}, bf16[2,1280,256]{1,2,0:T(8,128)(2,1)}, s32[2]{0:T(128)S(1)}, s32[]{:T(128)}, /*index=5*/bf16[...) while((s32[]{:T(128)}, bf16[2,512,512]{2,1,0:T(8,128)(2,1)}, ...), condition=%wide.region_3.4_spmd, body=%wide.region_0.3_spmd.sunk | while | flops 845295104 | bytes 101627824 | solution.py:66
  22.7 0.6 dynamic_slice.27
  24.0 0.8 fusion.39
  24.8 1.4 fusion.37
  26.2 1.0 constant_dynamic-slice_fusion.5
  27.2 1.1 constant_dynamic-slice_fusion.6
  28.2 0.2 copy.45
  28.5 7.6 %fusion.40 = (f32[4,2,512]{2,1,0:T(2,128)S(1)}, f32[4,768,512,2]{2,1,3,0:T(8,128)}) fusion(pred[512,768]{0,1:T(8,128)(4,1)S(1)} %fusion.39, bf16[768,4,64,1]{0,2,3,1:T(8,128)(2,1)} %bitcast.65, bf16[512,4,2,64]{0,3,2,1:T(8,128)(2,1)S(1)} %bitcast.64), kind=kOutput, calls=%fused_computation.4.clone.1 | convolution fusion | flops 412086272 | bytes 13910016 | tf_op jit(solution)/shard_map/while/body/eval_jaxpr/qhgd,khd->hgqk/dot_general | solution.py:48
  36.1 0.1 copy.46
  36.2 0.1 broadcast_maximum_fusion.2
  36.2 7.3 %fusion.41 = f32[4,2,512]{2,1,0:T(2,128)S(1)} fusion(f32[4,768,512,2]{2,1,3,0:T(8,128)} %get-tuple-element.197, f32[4,2,512]{2,1,0:T(2,128)S(1)} %broadcast_maximum_fusion.2, pred[512,768]{0,1:T(8,128)(4,1)S(1)} %fusion.39), kind=kLoop, calls=%fused_computation.3.clone.1 | loop fusion | flops 12578816 | bytes 13008896 | tf_op jit(solution)/shard_map/while/body/eval_jaxpr/reduce_sum | solution.py:61
  43.6 0.1 exponential_add_fusion.2
  43.7 0.7 copy-done.1
  44.4 3.6 fusion.42
  48.0 0.2 copy.47
  48.2 0.8 constant_dynamic-update-slice_fusion.2
  49.0 0.6 dynamic_slice.27
  50.3 0.8 fusion.39
  51.1 1.4 fusion.37
  52.5 1.0 constant_dynamic-slice_fusion.5
  53.5 1.1 constant_dynamic-slice_fusion.6
  54.5 0.2 copy.45
  54.8 7.6 %fusion.40 = (f32[4,2,512]{2,1,0:T(2,128)S(1)}, f32[4,768,512,2]{2,1,3,0:T(8,128)}) fusion(pred[512,768]{0,1:T(8,128)(4,1)S(1)} %fusion.39, bf16[768,4,64,1]{0,2,3,1:T(8,128)(2,1)} %bitcast.65, bf16[512,4,2,64]{0,3,2,1:T(8,128)(2,1)S(1)} %bitcast.64), kind=kOutput, calls=%fused_computation.4.clone.1 | convolution fusion | flops 412086272 | bytes 13910016 | tf_op jit(solution)/shard_map/while/body/eval_jaxpr/qhgd,khd->hgqk/dot_general | solution.py:48
  62.4 0.1 copy.46
  62.5 0.1 broadcast_maximum_fusion.2
  62.5 7.3 %fusion.41 = f32[4,2,512]{2,1,0:T(2,128)S(1)} fusion(f32[4,768,512,2]{2,1,3,0:T(8,128)} %get-tuple-element.197, f32[4,2,512]{2,1,0:T(2,128)S(1)} %broadcast_maximum_fusion.2, pred[512,768]{0,1:T(8,128)(4,1)S(1)} %fusion.39), kind=kLoop, calls=%fused_computation.3.clone.1 | loop fusion | flops 12578816 | bytes 13008896 | tf_op jit(solution)/shard_map/while/body/eval_jaxpr/reduce_sum | solution.py:61
  69.9 0.1 exponential_add_fusion.2
  70.0 0.7 copy-done.1
  70.7 3.6 fusion.42
  74.3 0.2 copy.47
  74.5 0.8 constant_dynamic-update-slice_fusion.2
  75.3 5.5 %convolution_convert_fusion.1 = bf16[1024,2048]{1,0:T(8,128)(2,1)} fusion(bf16[1024,512]{1,0:T(8,128)(2,1)} %bitcast.71, bf16[512,2048]{1,0:T(8,128)(2,1)S(1)} %copy-done), kind=kOutput, calls=%fused_computation.24 | convolution fusion | flops 2149580800 | bytes 7340032 | tf_op jit(solution)/shard_map/dot_general | solution.py:98
  80.9 0.0 reduce-scatter.3.cloned.1.call-update
  80.9 0.0 all-gather.9.cloned.1.call-start
  80.9 0.5 all-gather.9.cloned.1.call-update
  81.5 0.0 copy-start.7
  81.5 0.0 all-gather.7.cloned.1.call-start
  81.5 0.5 all-gather.7.cloned.1.call-update
  82.1 0.0 all-gather.5.cloned.1.call-start
  82.1 44.6 %reduce-scatter.3.cloned.1.call-done = bf16[256,2048]{1,0:T(8,128)(2,1)} async-done(((bf16[1024,2048]{1,0:T(8,128)(2,1)}), bf16[256,2048]{1,0:T(8,128)(2,1)}) %reduce-scatter.3.cloned.1.call-update) | async-done | bytes 1048592 | tf_op jit(solution)/shard_map/reduce_scatter | solution.py:97
  126.7 1.7 fusion.11
  128.4 0.5 multiply_reduce_fusion.1
  129.0 1.5 add_convert_fusion.1
  130.5 0.0 all-gather.5.cloned.1.call-update
  130.5 0.2 reduce-scatter.5.cloned.1.call-start
  130.8 78.1 %all-gather.9.cloned.1.call-done = bf16[16384,256]{1,0:T(8,128)(2,1)} async-done(((bf16[2048,256]{1,0:T(8,128)(2,1)}), bf16[16384,256]{1,0:T(8,128)(2,1)}) %all-gather.9.cloned.1.call-update) | async-done | bytes 8388624 | tf_op jit(solution)/shard_map/all_gather | solution.py:90
  208.8 11.7 %copy.35 = bf16[2048,8,256]{0,2,1:T(8,128)(2,1)} copy(bf16[2048,8,256]{2,0,1:T(8,128)(2,1)} %bitcast.68) | data formatting | bytes 16777216 | tf_op jit(solution)/shard_map/reshape | solution.py:90
  220.6 112.6 %all-gather.7.cloned.1.call-done = bf16[2048,2048]{1,0:T(8,128)(2,1)} async-done(((bf16[256,2048]{1,0:T(8,128)(2,1)}), bf16[2048,2048]{1,0:T(8,128)(2,1)}) %all-gather.7.cloned.1.call-update) | async-done | bytes 8388624 | tf_op jit(solution)/shard_map/all_gather | solution.py:89
  333.2 34.0 %all-gather.5.cloned.1.call-done = bf16[1024,2048]{1,0:T(8,128)(2,1)} async-done(((bf16[256,2048]{1,0:T(8,128)(2,1)}), bf16[1024,2048]{1,0:T(8,128)(2,1)}) %all-gather.5.cloned.1.call-update) | async-done | bytes 4194320 | tf_op jit(solution)/shard_map/all_gather | solution.py:107
  367.1 25.4 %convolution_convert_fusion = bf16[1024,2048]{1,0:T(8,128)(2,1)} fusion(bf16[2048,2048]{0,1:T(8,128)(2,1)} %bitcast.69, bf16[1024,2048]{1,0:T(8,128)(2,1)} %all-gather.5.cloned.1.call-done, bf16[2048,2048]{1,0:T(8,128)(2,1)} %all-gather.7.cloned.1.call-done), kind=kOutput, calls=%fused_computation.23 | convolution fusion | flops 17188257792 | bytes 25165824 | tf_op jit(solution)/shard_map/dot_general | solution.py:110
  392.5 0.0 reduce-scatter.5.cloned.1.call-update
  392.6 44.7 %reduce-scatter.5.cloned.1.call-done = bf16[256,2048]{1,0:T(8,128)(2,1)} async-done(((bf16[1024,2048]{1,0:T(8,128)(2,1)}), bf16[256,2048]{1,0:T(8,128)(2,1)}) %reduce-scatter.5.cloned.1.call-update) | async-done | bytes 1048592 | tf_op jit(solution)/shard_map/reduce_scatter | solution.py:109
  437.3 1.7 fusion.13
  439.0 0.5 multiply_reduce_fusion
  439.5 1.5 add_convert_fusion
  (38 shorter events, 0.1 us)
Async XLA Ops:
  7.4 68.0 %copy-start = (bf16[512,2048]{1,0:T(8,128)(2,1)S(1)}, bf16[512,2048]{1,0:T(8,128)(2,1)}, u32[]{:S(2)}) copy-start(bf16[512,2048]{1,0:T(8,128)(2,1)} %param.17) | copy-start | bytes 6291460
  7.4 8.6 %copy-start.11 = (f32[8]{0:T(128)S(1)}, f32[8]{0:T(128)}, u32[]{:S(2)}) copy-start(f32[8]{0:T(128)} %param.16) | copy-start | bytes 100
  7.4 119.3 %reduce-scatter.3.cloned.1.call-start = ((), (), s32[]{:S(2)}) async-start(), calls=%async_computation.2 | async-start | bytes 5242880 | tf_op jit(solution)/shard_map/reduce_scatter | solution.py:97
  9.7 7.9 %collective-permute-start = (bf16[2,128,256]{1,2,0:T(8,128)(2,1)}, bf16[2,128,256]{1,2,0:T(8,128)(2,1)S(1)}, u32[]{:S(2)}, u32[]{:S(2)}) collective-permute-start(bf16[2,128,256]{1,2,0:T(8,128)(2,1)} %get-tuple-element.138), channel_id=1, source_target_pairs={{0,4},{4,8},{8,12},{12,16},{16,20},{20,24},{24,28},{1,5},{5,9},{9,... | collective-permute-start | bytes 393224 | tf_op jit(solution)/shard_map/ppermute | solution.py:17
  14.6 6.9 %collective-permute-start.1 = (bf16[2,128,256]{1,2,0:T(8,128)(2,1)S(1)}, bf16[2,128,256]{1,2,0:T(8,128)(2,1)S(1)}, u32[]{:S(2)}, u32[]{:S(2)}) collective-permute-start(bf16[2,128,256]{1,2,0:T(8,128)(2,1)S(1)} %get-tuple-element.139), channel_id=1, source_target_pairs={{4,0},{8,4},{12,8},{16,12},{20,16},{24,20},{28,24},{5,1},{9,5},{13... | collective-permute-start | bytes 393224 | tf_op jit(solution)/shard_map/ppermute | solution.py:18
  36.2 8.2 %copy-start.1 = (f32[4,768,512,2]{2,1,3,0:T(8,128)S(1)}, f32[4,768,512,2]{2,1,3,0:T(8,128)}, u32[]{:S(2)}) copy-start(f32[4,768,512,2]{2,1,3,0:T(8,128)} %get-tuple-element.197) | copy-start | bytes 37748740 | tf_op jit(solution)/shard_map/while
  36.2 8.2 %copy-start.3 = (bf16[1,768,256]{1,2,0:T(8,128)(2,1)S(1)}, bf16[1,768,256]{1,2,0:T(8,128)(2,1)}, u32[]{:S(2)}) copy-start(bf16[1,768,256]{1,2,0:T(8,128)(2,1)} %get-tuple-element.193) | copy-start | bytes 1179652 | tf_op jit(solution)/shard_map/while
  62.5 8.2 %copy-start.1 = (f32[4,768,512,2]{2,1,3,0:T(8,128)S(1)}, f32[4,768,512,2]{2,1,3,0:T(8,128)}, u32[]{:S(2)}) copy-start(f32[4,768,512,2]{2,1,3,0:T(8,128)} %get-tuple-element.197) | copy-start | bytes 37748740 | tf_op jit(solution)/shard_map/while
  62.5 8.2 %copy-start.3 = (bf16[1,768,256]{1,2,0:T(8,128)(2,1)S(1)}, bf16[1,768,256]{1,2,0:T(8,128)(2,1)}, u32[]{:S(2)}) copy-start(bf16[1,768,256]{1,2,0:T(8,128)(2,1)} %get-tuple-element.193) | copy-start | bytes 1179652 | tf_op jit(solution)/shard_map/while
  80.8 45.9 %copy-start.4 = (bf16[256,2048]{1,0:T(8,128)(2,1)S(1)}, bf16[256,2048]{1,0:T(8,128)(2,1)}, u32[]{:S(2)}) copy-start(bf16[256,2048]{1,0:T(8,128)(2,1)} %param.13) | copy-start | bytes 3145732
  80.9 127.9 %all-gather.9.cloned.1.call-start = ((), (), s32[]{:S(2)}) async-start(), calls=%async_computation.6 | async-start | bytes 9437184 | tf_op jit(solution)/shard_map/all_gather | solution.py:90
  81.5 47.5 %copy-start.7 = (f32[2048]{0:T(1024)S(1)}, f32[2048]{0:T(1024)}, u32[]{:S(2)}) copy-start(f32[2048]{0:T(1024)} %param.19) | copy-start | bytes 24580
  81.5 47.5 %copy-start.8 = (f32[2048]{0:T(1024)S(1)}, f32[2048]{0:T(1024)}, u32[]{:S(2)}) copy-start(f32[2048]{0:T(1024)} %param.18) | copy-start | bytes 24580
  81.5 251.7 %all-gather.7.cloned.1.call-start = ((), (), s32[]{:S(2)}) async-start(), calls=%async_computation.4 | async-start | bytes 9437184 | tf_op jit(solution)/shard_map/all_gather | solution.py:89
  82.1 285.1 %all-gather.5.cloned.1.call-start = ((), (), s32[]{:S(2)}) async-start(), calls=%async_computation.3 | async-start | bytes 5242880 | tf_op jit(solution)/shard_map/all_gather | solution.py:107
  126.7 1.7 copy-start.5
  130.5 306.8 %reduce-scatter.5.cloned.1.call-start = ((), (), s32[]{:S(2)}) async-start(), calls=%async_computation.5 | async-start | bytes 5242880 | tf_op jit(solution)/shard_map/reduce_scatter | solution.py:109
  392.5 44.8 %copy-start.2 = (bf16[256,2048]{1,0:T(8,128)(2,1)S(1)}, bf16[256,2048]{1,0:T(8,128)(2,1)}, u32[]{:S(2)}) copy-start(bf16[256,2048]{1,0:T(8,128)(2,1)} %add_convert_fusion.1) | copy-start | bytes 3145732
  392.5 47.0 %copy-start.9 = (f32[2048]{0:T(1024)S(1)}, f32[2048]{0:T(1024)}, u32[]{:S(2)}) copy-start(f32[2048]{0:T(1024)} %param.23) | copy-start | bytes 24580
  392.5 47.0 %copy-start.10 = (f32[2048]{0:T(1024)S(1)}, f32[2048]{0:T(1024)}, u32[]{:S(2)}) copy-start(f32[2048]{0:T(1024)} %param.22) | copy-start | bytes 24580
  437.3 1.7 copy-start.6
Sparse Core Ops, SparseCore 0:
  81.0 45.6 reduce-scatter.2
  392.7 44.5 reduce-scatter.4
Sparse Core Ops, SparseCore 1:
  83.5 125.3 all-gather.8
  210.8 122.3 all-gather.6
  334.6 32.5 all-gather.4
